TPU v7x, 512 devices: a 4x2x32 block of a 4x8x32 slice. The times are simulated.
512 devices in a mesh: grp: 2 (over y), sp: 64 (over z, core), tp: 4 (over x).
Axes of the slice: x: 4, y: 2, z: 32, core: 2. Of those that a mesh axis runs over, the one named last changes fastest.
The devices are a block of a 4x8x32 slice.
Arguments:
- tokens: bfloat16 [32768, 2048], P(('grp', 'sp'), 'tp'), parts along dimension 0, may hold values from -6 to 6
- norm_gain: float32 [2048], replicated, may hold values from 0.1 to 1.9
- ret_query_weight: bfloat16 [2048, 256], P('sp', 'tp'), may hold values from -0.125 to 0.125
- ret_key_weight: bfloat16 [2048, 256], P('sp', 'tp'), may hold values from -0.125 to 0.125
- ret_value_weight: bfloat16 [2048, 512], P('sp', 'tp'), may hold values from -0.125 to 0.125
- fox_query_weight: bfloat16 [2048, 512], P('sp', 'tp'), may hold values from -8 to 8
- fox_key_weight: bfloat16 [2048, 512], P('sp', 'tp'), may hold values from -0.125 to 0.125
- fox_value_weight: bfloat16 [2048, 512], P('sp', 'tp'), may hold values from -0.125 to 0.125
- ret_decay: float32 [8], P('tp'), may hold values from -1 to 0, as said below
- ret_state: float32 [16, 32, 64], P(('grp', 'tp')), parts along dimension 0, may hold values from -256 to 256
- head_norm_gain: float32 [512], P('tp'), may hold values from 0.1 to 1.9
- fox_gates: float32 [32768, 8], P('grp', 'tp'), parts along dimension 0, may hold values from -49152 to 0, as said below
- ret_out_weight: bfloat16 [512, 2048], P('tp', 'sp'), may hold values from -0.1875 to 0.1875
- fox_out_weight: bfloat16 [512, 2048], P('tp', 'sp'), may hold values from -1 to 1
Outputs:
- mixed: bfloat16 [32768, 2048], P(('grp', 'sp', 'tp')), parts along dimension 0
There are 2 independent parts, one for each index of `grp`. A program takes and returns all parts, laid end to end along the dimension named above; an argument that names none is the same for every part. Nothing has to cross between parts.
Inputs may be any that keep to these rules, and one draw needn't show every extreme that they name: `ret_decay`: each head's log decay is negative. `fox_gates`: along the positions each head's column never rises.
All inputs are finite; a program needn't handle non-finite values.
Results may differ from a plain program's by a relative error of at most 0.015.
The roundings to bfloat16 on the way count: a program that leaves them out, or rounds other values in their place, can miss the bound.
Values may be sent and summed in bfloat16 or wider, within the bound.
No kernel may reach another device: no remote copies, remote signals or barrier semaphores. Data moves between devices by JAX's collectives and lax.ppermute only.
A program may use at most 64 MiB of HBM per device.

v0:
```python
import jax
import jax.numpy as jnp
from jax import lax
from jax.sharding import Mesh
from jax.sharding import PartitionSpec as P

SP = ("sp_0", "sp_1")
GRP_SP = ("grp", "sp_0", "sp_1")
GRP_SP_TP = ("grp", "sp_0", "sp_1", "tp")
epsilon = 1e-06


def in_order(blocks, dim):
    shape = list(blocks.shape[1:])
    shape[dim] *= blocks.shape[0]
    return jnp.moveaxis(blocks, 0, dim).reshape(shape)


def from_everyone(array, axis):
    count = lax.axis_size(axis)
    return lax.all_to_all(
        jnp.broadcast_to(array[None], (count, *array.shape)), axis, 0, 0, tiled=True
    )


def collect_2(array, axis, dim):
    return in_order(from_everyone(array, axis), dim)


def sent_together(arrays, axis, dim, along):
    widths = [a.shape[along] for a in arrays]
    both = jnp.concatenate(arrays, axis=along)
    result = lax.all_gather(both, axis, axis=dim, tiled=True)
    return tuple(jnp.split(result, [sum(widths[:k]) for k in range(1, len(widths))], axis=along))


def all_blocks(array, axes, order):
    blocks = array
    for k in order:
        blocks = lax.all_gather(blocks, axes[k])
    done = order[::-1]
    back = [done.index(k) for k in range(len(axes))]
    blocks = blocks.transpose(*back, *range(len(axes), blocks.ndim))
    return blocks.reshape(-1, *array.shape)


def whole_of(array, axes, order, dim):
    return in_order(all_blocks(array, axes, order), dim)


def rows_first(arrays, axis, dims):
    turned = [jnp.moveaxis(a, dim, 0) for a, dim in zip(arrays, dims)]
    both = jnp.concatenate([t.reshape(len(t), -1) for t in turned], axis=1)
    result, at, gathered = (lax.all_gather(both, axis, axis=0, tiled=True), 0, [])
    for t, dim in zip(turned, dims):
        piece = result[:, at : at + t[0].size].reshape(-1, *t.shape[1:])
        gathered.append(jnp.moveaxis(piece, 0, dim))
        at += t[0].size
    return tuple(gathered)


def in_blocks(array, dim, count):
    before, after = (array.shape[:dim], array.shape[dim + 1 :])
    return jnp.moveaxis(array.reshape(*before, count, -1, *after), dim, 0)


def summed_on_arrival(array, axis, dim):
    blocks = in_blocks(array, dim, lax.axis_size(axis))
    arrived = lax.all_to_all(blocks, axis, split_axis=0, concat_axis=0, tiled=True)
    return arrived.astype(jnp.float32).sum(axis=0)


def head_group_norm(joined_output, norm_gains):
    center = joined_output - jnp.mean(joined_output, axis=-1, keepdims=True)
    spread = jnp.mean(center * center, axis=-1, keepdims=True)
    normal = (
        center
        * lax.rsqrt(spread + epsilon)
        * norm_gains.reshape(joined_output.shape[1], joined_output.shape[2])
    )
    return normal.reshape(joined_output.shape[0], -1).astype(jnp.bfloat16)


def softmax_update(
    current,
    query_heads,
    query_gates,
    query_pos,
    key_block,
    value_block,
    gate_block,
    key_pos,
    score_scale,
):
    top_now, total_now, weighted = current
    logits = (
        jnp.einsum("qhd,khd->hqk", query_heads, key_block, preferred_element_type=jnp.float32)
        * score_scale
    )
    logits = logits + query_gates[:, :, None] - gate_block[:, None, :]
    logits = jnp.where(key_pos[None, None, :] <= query_pos[None, :, None], logits, -jnp.inf)
    top_new = jnp.maximum(top_now, jnp.max(logits, axis=-1))
    weights_new = jnp.exp(logits - top_new[:, :, None])
    rescale = jnp.exp(top_now - top_new)
    total_new = total_now * rescale + jnp.sum(weights_new, axis=-1)
    weighted_new = weighted * rescale[:, :, None] + jnp.einsum(
        "hqk,khd->hqd",
        weights_new.astype(jnp.bfloat16),
        value_block,
        preferred_element_type=jnp.float32,
    )
    return (top_new, total_new, weighted_new)


def local(
    tokens,
    norm_gain,
    ret_query_weight,
    ret_key_weight,
    ret_value_weight,
    fox_query_weight,
    fox_key_weight,
    fox_value_weight,
    ret_decay,
    ret_state,
    head_norm_gain,
    fox_gates,
    ret_out_weight,
    fox_out_weight,
):
    sequence_length = tokens.shape[0]
    gathered = collect_2(tokens, "tp", 1)
    widened = gathered.astype(jnp.float32)
    normed = (
        widened
        * lax.rsqrt(jnp.mean(widened * widened, axis=-1, keepdims=True) + epsilon)
        * norm_gain
    ).astype(jnp.bfloat16)
    portions = sent_together(
        (
            ret_query_weight,
            ret_key_weight,
            ret_value_weight,
            fox_query_weight,
            fox_key_weight,
            fox_value_weight,
        ),
        SP,
        0,
        1,
    )
    sums = tuple(
        (jnp.dot(normed, portion, preferred_element_type=jnp.float32) for portion in portions)
    )
    ret_query, ret_key, ret_value, fox_query, fox_key, fox_value = [
        result.astype(jnp.bfloat16) for result in sums
    ]
    ret_heads = ret_decay.shape[0]
    key_size = ret_query.shape[1] // ret_heads
    value_size = ret_value.shape[1] // ret_heads
    place = lax.axis_index(SP)
    offset = place * sequence_length
    queries = ret_query.astype(jnp.float32).reshape(sequence_length, ret_heads, key_size)
    keys_local = ret_key.astype(jnp.float32).reshape(
        sequence_length, ret_heads, key_size
    ) * key_size ** (-0.5)
    values_local = ret_value.astype(jnp.float32).reshape(sequence_length, ret_heads, value_size)
    positions = jnp.arange(sequence_length, dtype=jnp.float32)
    spread = positions[:, None] - positions[None, :]
    within = jnp.where(
        spread[None] >= 0, jnp.exp(jnp.maximum(spread, 0.0)[None] * ret_decay[:, None, None]), 0.0
    )
    leading = jnp.exp((positions + 1.0)[:, None] * ret_decay[None, :])
    trailing = jnp.exp((sequence_length - 1.0 - positions)[:, None] * ret_decay[None, :])
    scores = jnp.einsum("ihd,jhd->hij", queries, keys_local) * within
    inner_value = jnp.einsum("hij,jhe->ihe", scores, values_local)
    summary = jnp.einsum("jhd,jhe->hde", keys_local * trailing[:, :, None], values_local)
    portion = whole_of(summary[None], SP, (0, 1), 0)
    shard_ids = jnp.arange(portion.shape[0], dtype=jnp.int32)
    distance = jnp.maximum(place - shard_ids - 1, 0).astype(jnp.float32) * sequence_length
    weight = jnp.where(
        (shard_ids < place)[:, None], jnp.exp(distance[:, None] * ret_decay[None, :]), 0.0
    )
    before = jnp.einsum("sh,shde->hde", weight, portion)
    entering = jnp.exp(offset.astype(jnp.float32) * ret_decay)[:, None, None] * ret_state + before
    carried_state = jnp.einsum("ihd,hde->ihe", queries, entering) * leading[:, :, None]
    retention_mixed = head_group_norm(inner_value + carried_state, head_norm_gain)
    fox_heads = fox_gates.shape[1]
    head_size = fox_query.shape[1] // fox_heads
    score_scale = head_size ** (-0.5)
    starting = (
        jnp.full((fox_heads, sequence_length), -1e30, jnp.float32),
        jnp.zeros((fox_heads, sequence_length), jnp.float32),
        jnp.zeros((fox_heads, sequence_length, head_size), jnp.float32),
    )
    query_heads = fox_query.reshape(sequence_length, fox_heads, head_size)
    own_gates = lax.dynamic_slice_in_dim(fox_gates, offset, sequence_length, 0).T
    query_pos = offset + jnp.arange(sequence_length, dtype=jnp.int32)
    last_query = offset + sequence_length - 1

    def attend(running, portion, first_key):
        key_rows, value_rows = portion
        count = key_rows.shape[0]
        block_rows = next(
            (candidate for candidate in (2048, 1024, 512) if count % candidate == 0), count
        )

        def advance(state_now, number):
            key_start = first_key + number * block_rows

            def compute(current):
                key_block = lax.dynamic_slice_in_dim(
                    key_rows, number * block_rows, block_rows, 0
                ).reshape(block_rows, fox_heads, head_size)
                value_block = lax.dynamic_slice_in_dim(
                    value_rows, number * block_rows, block_rows, 0
                ).reshape(block_rows, fox_heads, head_size)
                gate_block = lax.dynamic_slice_in_dim(fox_gates, key_start, block_rows, 0).T
                key_pos = key_start + jnp.arange(block_rows, dtype=jnp.int32)
                return softmax_update(
                    current,
                    query_heads,
                    own_gates,
                    query_pos,
                    key_block,
                    value_block,
                    gate_block,
                    key_pos,
                    score_scale,
                )

            def unchanged(current):
                return current

            return (lax.cond(key_start <= last_query, compute, unchanged, state_now), None)

        finished, _ = lax.scan(advance, running, jnp.arange(count // block_rows, dtype=jnp.int32))
        return finished

    top_final, total_final, weighted_final = attend(
        starting, sent_together((fox_key, fox_value), SP, 0, 1), jnp.int32(0)
    )
    fox_mix = (
        jnp.transpose(weighted_final / total_final[:, :, None], (1, 0, 2))
        .reshape(sequence_length, fox_heads * head_size)
        .astype(jnp.bfloat16)
    )
    ret_full, fox_full = rows_first((ret_out_weight, fox_out_weight), SP, (1, 1))
    mixed = summed_on_arrival(
        (
            jnp.dot(retention_mixed, ret_full, preferred_element_type=jnp.float32)
            + jnp.dot(fox_mix, fox_full, preferred_element_type=jnp.float32)
        ).astype(jnp.bfloat16),
        "tp",
        0,
    )
    return mixed.astype(jnp.bfloat16)


def solution(mesh):
    torus = Mesh(
        mesh.devices.reshape(mesh.shape["grp"], 32, 2, mesh.shape["tp"]),
        ("grp", "sp_0", "sp_1", "tp"),
    )
    return jax.shard_map(
        local,
        mesh=torus,
        in_specs=(
            P(GRP_SP, "tp"),
            P(),
            P(SP, "tp"),
            P(SP, "tp"),
            P(SP, "tp"),
            P(SP, "tp"),
            P(SP, "tp"),
            P(SP, "tp"),
            P("tp"),
            P(("grp", "tp"), None, None),
            P("tp"),
            P("grp", "tp"),
            P("tp", SP),
            P("tp", SP),
        ),
        out_specs=P(GRP_SP_TP, None),
        check_vma=False,
    )
```

profile of v0, /device:TPU:1824, one launch (start us, length us, event | category | flops | bytes accessed | tf_op | source)
XLA Modules:
  0.0 499.1 jit_solution(9401134259431210037)
XLA Ops:
  6.6 1.5 concatenate.9
  10.3 4.6 all-to-all-start
  15.7 14.3 %all-to-all-done = bf16[4,256,512]{1,2,0:T(8,128)(2,1)S(1)} async-done(((bf16[4,256,512]{1,2,0:T(8,128)(2,1)}), bf16[4,256,512]{1,2,0:T(8,128)(2,1)S(1)}, u32[]{:S(2)}, u32[]{:S(2)}) %all-to-all-start) | async-done | bytes 1048608 | tf_op jit(solution)/shard_map/all_to_all | solution.py:21
  30.7 99.2 %all-gather.6.cloned.1.call-done = bf16[2048,640]{1,0:T(8,128)(2,1)} async-done(((bf16[32,640]{1,0:T(8,128)(2,1)}), bf16[2048,640]{1,0:T(8,128)(2,1)}) %all-gather.6.cloned.1.call-update) | async-done | bytes 2621456 | tf_op jit(solution)/shard_map/all_gather | solution.py:33
  134.7 1.6 convolution_convert_fusion.4
  137.9 56.2 %all-gather = bf16[64,32,64]{2,1,0:T(8,128)(2,1)S(1)} all-gather(bf16[2,32,64]{2,1,0:T(8,128)(2,1)S(1)} %fusion.37), channel_id=2, replica_groups=mesh['grp'=2,'sp_0'=32,'sp_1'=2,'tp'=4] {'sp_0'}, dimensions={0}, use_global_device_ids=true | all-gather | bytes 270336 | tf_op jit(solution)/shard_map/all_gather | solution.py:40
  194.0 2.6 all-gather.1
  199.6 1.4 convolution_convert_fusion
  201.0 56.6 %all-gather.8.cloned.1.call-done = bf16[2048,256]{1,0:T(8,128)(2,1)} async-done(((bf16[32,256]{1,0:T(8,128)(2,1)}), bf16[2048,256]{1,0:T(8,128)(2,1)}) %all-gather.8.cloned.1.call-update) | async-done | bytes 1048592 | tf_op jit(solution)/shard_map/all_gather | solution.py:54
  257.7 1.5 fusion.23
  259.2 148.0 %all-gather.10.cloned.1.call-done = bf16[16384,256]{0,1:T(8,128)(2,1)} async-done(((bf16[256,256]{0,1:T(8,128)(2,1)}), bf16[16384,256]{0,1:T(8,128)(2,1)}) %all-gather.10.cloned.1.call-update) | async-done | bytes 8388624 | tf_op jit(solution)/shard_map/all_gather | solution.py:33
  407.2 5.8 %fusion.48 = (bf16[16384,128]{0,1:T(8,128)(2,1)}, bf16[16384,128]{0,1:T(8,128)(2,1)}) fusion(bf16[16384,256]{0,1:T(8,128)(2,1)} %all-gather.10.cloned.1.call-done), kind=kLoop, calls=%fused_computation.83 | loop fusion | bytes 16777216 | tf_op jit(solution)/shard_map/split | solution.py:34
  413.0 58.6 %while.15 = (s32[]{:T(128)}, f32[2,256]{1,0:T(2,128)S(1)}, f32[2,256]{1,0:T(2,128)S(1)}, f32[2,256,64]{1,2,0:T(8,128)S(1)}, s32[8]{0:T(128)S(1)}, /*index=5*/s32...) while((s32[]{:T(128)}, f32[2,256]{1,0:T(2,128)S(1)}, ...), condition=%wide.region_8.9_spmd.clone, body=%wide.region_3.8_spmd.clone.sunk | while | flops 278465792 | bytes 17209772 | solution.py:237
  414.3 6.0 %conditional.3 = ((f32[2,256]{1,0:T(2,128)S(1)}, f32[2,256]{1,0:T(2,128)S(1)}, f32[2,256,64]{1,2,0:T(8,128)S(1)})) conditional(s32[]{:T(128)} %convert_element_type.113, (f32[2,256]{1,0:T(2,128)S(1)}, f32[2,256]{1,0:T(2,128)S(1)}, f32[2,256,64]{1,2,0:T(8,128)S(1)}) %tuple.39, (s32[]{:T(128)}, s32[]{:T(128)}, s32[]{:T(128)}, ...), branch_computations={%region_4.4_spmd, %region_5.7_spmd} | conditional | flops 278465792 | bytes 17208448 | solution.py:235
  421.6 6.1 %conditional.3 = ((f32[2,256]{1,0:T(2,128)S(1)}, f32[2,256]{1,0:T(2,128)S(1)}, f32[2,256,64]{1,2,0:T(8,128)S(1)})) conditional(s32[]{:T(128)} %convert_element_type.113, (f32[2,256]{1,0:T(2,128)S(1)}, f32[2,256]{1,0:T(2,128)S(1)}, f32[2,256,64]{1,2,0:T(8,128)S(1)}) %tuple.39, (s32[]{:T(128)}, s32[]{:T(128)}, s32[]{:T(128)}, ...), branch_computations={%region_4.4_spmd, %region_5.7_spmd} | conditional | flops 278465792 | bytes 17208448 | solution.py:235
  424.9 1.4 fusion.47
  429.0 6.0 %conditional.3 = ((f32[2,256]{1,0:T(2,128)S(1)}, f32[2,256]{1,0:T(2,128)S(1)}, f32[2,256,64]{1,2,0:T(8,128)S(1)})) conditional(s32[]{:T(128)} %convert_element_type.113, (f32[2,256]{1,0:T(2,128)S(1)}, f32[2,256]{1,0:T(2,128)S(1)}, f32[2,256,64]{1,2,0:T(8,128)S(1)}) %tuple.39, (s32[]{:T(128)}, s32[]{:T(128)}, s32[]{:T(128)}, ...), branch_computations={%region_4.4_spmd, %region_5.7_spmd} | conditional | flops 278465792 | bytes 17208448 | solution.py:235
  436.3 6.1 %conditional.3 = ((f32[2,256]{1,0:T(2,128)S(1)}, f32[2,256]{1,0:T(2,128)S(1)}, f32[2,256,64]{1,2,0:T(8,128)S(1)})) conditional(s32[]{:T(128)} %convert_element_type.113, (f32[2,256]{1,0:T(2,128)S(1)}, f32[2,256]{1,0:T(2,128)S(1)}, f32[2,256,64]{1,2,0:T(8,128)S(1)}) %tuple.39, (s32[]{:T(128)}, s32[]{:T(128)}, s32[]{:T(128)}, ...), branch_computations={%region_4.4_spmd, %region_5.7_spmd} | conditional | flops 278465792 | bytes 17208448 | solution.py:235
  439.6 1.4 fusion.47
  443.6 6.0 %conditional.3 = ((f32[2,256]{1,0:T(2,128)S(1)}, f32[2,256]{1,0:T(2,128)S(1)}, f32[2,256,64]{1,2,0:T(8,128)S(1)})) conditional(s32[]{:T(128)} %convert_element_type.113, (f32[2,256]{1,0:T(2,128)S(1)}, f32[2,256]{1,0:T(2,128)S(1)}, f32[2,256,64]{1,2,0:T(8,128)S(1)}) %tuple.39, (s32[]{:T(128)}, s32[]{:T(128)}, s32[]{:T(128)}, ...), branch_computations={%region_4.4_spmd, %region_5.7_spmd} | conditional | flops 278465792 | bytes 17208448 | solution.py:235
  451.0 6.1 %conditional.3 = ((f32[2,256]{1,0:T(2,128)S(1)}, f32[2,256]{1,0:T(2,128)S(1)}, f32[2,256,64]{1,2,0:T(8,128)S(1)})) conditional(s32[]{:T(128)} %convert_element_type.113, (f32[2,256]{1,0:T(2,128)S(1)}, f32[2,256]{1,0:T(2,128)S(1)}, f32[2,256,64]{1,2,0:T(8,128)S(1)}) %tuple.39, (s32[]{:T(128)}, s32[]{:T(128)}, s32[]{:T(128)}, ...), branch_computations={%region_4.4_spmd, %region_5.7_spmd} | conditional | flops 278465792 | bytes 17208448 | solution.py:235
  458.3 6.0 %conditional.3 = ((f32[2,256]{1,0:T(2,128)S(1)}, f32[2,256]{1,0:T(2,128)S(1)}, f32[2,256,64]{1,2,0:T(8,128)S(1)})) conditional(s32[]{:T(128)} %convert_element_type.113, (f32[2,256]{1,0:T(2,128)S(1)}, f32[2,256]{1,0:T(2,128)S(1)}, f32[2,256,64]{1,2,0:T(8,128)S(1)}) %tuple.39, (s32[]{:T(128)}, s32[]{:T(128)}, s32[]{:T(128)}, ...), branch_computations={%region_4.4_spmd, %region_5.7_spmd} | conditional | flops 278465792 | bytes 17208448 | solution.py:235
  465.6 6.0 %conditional.3 = ((f32[2,256]{1,0:T(2,128)S(1)}, f32[2,256]{1,0:T(2,128)S(1)}, f32[2,256,64]{1,2,0:T(8,128)S(1)})) conditional(s32[]{:T(128)} %convert_element_type.113, (f32[2,256]{1,0:T(2,128)S(1)}, f32[2,256]{1,0:T(2,128)S(1)}, f32[2,256,64]{1,2,0:T(8,128)S(1)}) %tuple.39, (s32[]{:T(128)}, s32[]{:T(128)}, s32[]{:T(128)}, ...), branch_computations={%region_4.4_spmd, %region_5.7_spmd} | conditional | flops 278465792 | bytes 17208448 | solution.py:235
  472.2 19.4 %all_to_all.10 = bf16[4,64,2048]{2,1,0:T(8,128)(2,1)S(1)} all-to-all(bf16[4,64,2048]{2,1,0:T(8,128)(2,1)S(1)} %bitcast.68), channel_id=1, replica_groups=mesh['grp'=2,'sp_0'=32,'sp_1'=2,'tp'=4] {'tp'}, dimensions={0} | all-to-all | bytes 2097152 | tf_op jit(solution)/shard_map/all_to_all | solution.py:69
  (160 shorter events, 58.8 us)
Async XLA Ops:
  6.5 8.3 %copy-start.3 = (bf16[128,32]{0,1:T(8,128)(2,1)S(1)}, bf16[128,32]{0,1:T(8,128)(2,1)}, u32[]{:S(2)}) copy-start(bf16[128,32]{0,1:T(8,128)(2,1)} %param.31) | copy-start | bytes 24580
  6.5 8.3 %copy-start.4 = (bf16[128,32]{0,1:T(8,128)(2,1)S(1)}, bf16[128,32]{0,1:T(8,128)(2,1)}, u32[]{:S(2)}) copy-start(bf16[128,32]{0,1:T(8,128)(2,1)} %param.30) | copy-start | bytes 24580
  6.6 23.8 %copy-start.2 = (f32[2048]{0:T(1024)S(1)}, f32[2048]{0:T(1024)}, u32[]{:S(2)}) copy-start(f32[2048]{0:T(1024)} %param.19) | copy-start | bytes 24580
  6.6 123.3 %all-gather.6.cloned.1.call-start = ((), (), s32[]{:S(2)}) async-start(), calls=%async_computation.2 | async-start | bytes 2662400 | tf_op jit(solution)/shard_map/all_gather | solution.py:33
  10.3 19.7 %all-to-all-start = ((bf16[4,256,512]{1,2,0:T(8,128)(2,1)}), bf16[4,256,512]{1,2,0:T(8,128)(2,1)S(1)}, u32[]{:S(2)}, u32[]{:S(2)}) async-start(bf16[4,256,512]{1,2,0:T(8,128)(2,1)} %broadcast_in_dim.40), calls=%async_computation | async-start | bytes 2097152 | tf_op jit(solution)/shard_map/all_to_all | solution.py:21
  14.8 242.8 %all-gather.8.cloned.1.call-start = ((), (), s32[]{:S(2)}) async-start(), calls=%async_computation.3 | async-start | bytes 1064960 | tf_op jit(solution)/shard_map/all_gather | solution.py:54
  15.6 391.6 %all-gather.10.cloned.1.call-start = ((), (), s32[]{:S(2)}) async-start(), calls=%async_computation.4 | async-start | bytes 8519680 | tf_op jit(solution)/shard_map/all_gather | solution.py:33
  30.3 103.1 %copy-start.6 = (f32[128]{0:T(128)S(1)}, f32[128]{0:T(128)}, u32[]{:S(2)}) copy-start(f32[128]{0:T(128)} %param.28) | copy-start | bytes 1540
  30.3 103.2 %copy-start.5 = (f32[2]{0:T(128)S(1)}, f32[2]{0:T(128)}, u32[]{:S(2)}) copy-start(f32[2]{0:T(128)} %param.26) | copy-start | bytes 28
  196.6 2.1 copy-start.1
  413.0 58.7 %copy-start = (bf16[2048,256]{1,0:T(8,128)(2,1)S(1)}, bf16[2048,256]{1,0:T(8,128)(2,1)}, u32[]{:S(2)}) copy-start(bf16[2048,256]{1,0:T(8,128)(2,1)} %all-gather.8.cloned.1.call-done) | copy-start | bytes 3145732
Sparse Core Ops, SparseCore 0:
  9.5 120.3 all-gather.5
  132.0 125.5 all-gather.7
  259.7 147.4 all-gather.9
where the time goes:
time: 501 us; the launch traced here: 499 us
  waiting for transfers between devices  318 us (63%)
  blocking collectives  78.2 us (16%)
  local copies, waits for them, and re-layouts  31.8 us (6%)
  matrix products  29.6 us (6%)
  between operations  13.3 us (3%)
  other arithmetic  11.7 us (2%)
  loops' own time  11.4 us (2%)
    all_gather x2, waiting for transfers between devices, sent_together(): result = lax.all_gather(both, axis, axis=dim, tiled=True)  247 us
    all_gather x2, blocking collectives, all_blocks(): blocks = lax.all_gather(blocks, axes[k])  58.8 us
    all_gather x1, waiting for transfers between devices, rows_first(): lax.all_gather(both, axis, axis=0, tiled=True)  56.6 us
    all_to_all x1, blocking collectives, summed_on_arrival(): lax.all_to_all(blocks, axis, split_axis=0, concat_axis=0, tiled=True)  19.4 us
    all_to_all x1, waiting for transfers between devices, from_everyone(): lax.all_to_all(jnp.broadcast_to(array[None], (count, *array.shape)), axis...  14.3 us
    dot_general x8, matrix products, softmax_update(): jnp.einsum('qhd,khd->hqk', query_heads, key_block, preferred_element_type...  11.2 us
    dynamic_slice x8, local copies, waits for them, and re-layouts, compute(): lax.dynamic_slice_in_dim(value_rows, number * block_rows, block_rows, 0)  10.2 us
  transfers between devices with their start and end apart: 4, of which 4 were waited for; matrix products, arithmetic and copies ran while one was open for 3% of the time, Pallas kernels for 0%

commit v1 on v0

--- a/solution.py
+++ b/solution.py
@@ -3,11 +3,18 @@
 from jax import lax
 from jax.sharding import Mesh
 from jax.sharding import PartitionSpec as P
+from jax.lax import all_to_all, axis_size
 
 SP = ("sp_0", "sp_1")
 GRP_SP = ("grp", "sp_0", "sp_1")
 GRP_SP_TP = ("grp", "sp_0", "sp_1", "tp")
 epsilon = 1e-06
+
+
+def local_data_pass(mesh_name, frame_in):
+    return jnp.concatenate(
+        all_to_all(jnp.stack([frame_in] * axis_size(mesh_name)), mesh_name, 0, 0), axis=0
+    )
 
 
 def in_order(blocks, dim):
@@ -51,7 +58,7 @@
 def rows_first(arrays, axis, dims):
     turned = [jnp.moveaxis(a, dim, 0) for a, dim in zip(arrays, dims)]
     both = jnp.concatenate([t.reshape(len(t), -1) for t in turned], axis=1)
-    result, at, gathered = (lax.all_gather(both, axis, axis=0, tiled=True), 0, [])
+    result, at, gathered = (local_data_pass(axis, both), 0, [])
     for t, dim in zip(turned, dims):
         piece = result[:, at : at + t[0].size].reshape(-1, *t.shape[1:])
         gathered.append(jnp.moveaxis(piece, 0, dim))

time: 501 us -> 453 us (0.904)
  the two profiles are of different devices: /device:TPU:1824 before, /device:TPU:1888 now
where the time goes in v1:
time: 453 us; the launch traced here: 452 us
  blocking collectives  192 us (42%)
  waiting for transfers between devices  146 us (32%)
  local copies, waits for them, and re-layouts  31.9 us (7%)
  matrix products  28.5 us (6%)
  starting transfers between devices  17.4 us (4%)
  between operations  13.7 us (3%)
  loops' own time  11.4 us (3%)
  other arithmetic  11.1 us (2%)
    all_gather x2, blocking collectives, all_blocks(): blocks = lax.all_gather(blocks, axes[k])  150 us
    all_gather x2, waiting for transfers between devices, sent_together(): result = lax.all_gather(both, axis, axis=dim, tiled=True)  146 us
    all_to_all x1, blocking collectives, summed_on_arrival(): lax.all_to_all(blocks, axis, split_axis=0, concat_axis=0, tiled=True)  22 us
    all_to_all x1, blocking collectives, from_everyone(): lax.all_to_all(jnp.broadcast_to(array[None], (count, *array.shape)), axis...  19.5 us
    all_to_all x1, starting transfers between devices, local_data_pass(): all_to_all(jnp.stack([frame_in] * axis_size(mesh_name)), mesh_name, 0, 0)  17.4 us
    dot_general x8, matrix products, softmax_update(): jnp.einsum('qhd,khd->hqk', query_heads, key_block, preferred_element_type...  11.2 us
    dynamic_slice x8, local copies, waits for them, and re-layouts, compute(): lax.dynamic_slice_in_dim(value_rows, number * block_rows, block_rows, 0)  10.2 us
  transfers between devices with their start and end apart: 3, of which 2 were waited for; matrix products, arithmetic and copies ran while one was open for 3% of the time, Pallas kernels for 0%

profile of v1, /device:TPU:1888, one launch (start us, length us, event | category | flops | bytes accessed | tf_op | source)
XLA Modules:
  0.0 451.7 jit_solution(16841999052273598982)
XLA Ops:
  6.6 1.5 concatenate.9
  9.3 19.5 %all_to_all.15 = bf16[4,256,512]{1,2,0:T(8,128)(2,1)S(1)} all-to-all(bf16[4,256,512]{1,2,0:T(8,128)(2,1)S(1)} %broadcast_in_dim.40), channel_id=1, replica_groups=mesh['grp'=2,'sp_0'=32,'sp_1'=2,'tp'=4] {'tp'}, dimensions={0} | all-to-all | bytes 2097152 | tf_op jit(solution)/shard_map/all_to_all | solution.py:28
  29.6 99.5 %all-gather.5.cloned.1.call-done = bf16[2048,640]{1,0:T(8,128)(2,1)} async-done(((bf16[32,640]{1,0:T(8,128)(2,1)}), bf16[2048,640]{1,0:T(8,128)(2,1)}) %all-gather.5.cloned.1.call-update) | async-done | bytes 2621456 | tf_op jit(solution)/shard_map/all_gather | solution.py:40
  130.5 1.4 convolution_convert_fusion.2
  133.8 17.4 %all-to-all-start.1 = ((bf16[64,32,256]{2,1,0:T(8,128)(2,1)}), bf16[64,32,256]{2,1,0:T(8,128)(2,1)S(1)}, u32[]{:S(2)}, u32[]{:S(2)}) async-start(bf16[64,32,256]{2,1,0:T(8,128)(2,1)} %stack.2), calls=%async_computation.1 | async-start | bytes 2097152 | tf_op jit(solution)/shard_map/all_to_all | solution.py:16
  152.4 1.6 convolution_convert_fusion.4
  155.6 147.4 %all-gather = bf16[64,32,64]{2,1,0:T(8,128)(2,1)S(1)} all-gather(bf16[2,32,64]{2,1,0:T(8,128)(2,1)S(1)} %fusion.37), channel_id=2, replica_groups=mesh['grp'=2,'sp_0'=32,'sp_1'=2,'tp'=4] {'sp_0'}, dimensions={0}, use_global_device_ids=true | all-gather | bytes 270336 | tf_op jit(solution)/shard_map/all_gather | solution.py:47
  303.0 2.7 all-gather.1
  310.5 46.4 %all-gather.7.cloned.1.call-done = bf16[16384,256]{0,1:T(8,128)(2,1)} async-done(((bf16[256,256]{0,1:T(8,128)(2,1)}), bf16[16384,256]{0,1:T(8,128)(2,1)}) %all-gather.7.cloned.1.call-update) | async-done | bytes 8388624 | tf_op jit(solution)/shard_map/all_gather | solution.py:40
  356.9 5.8 %fusion.48 = (bf16[16384,128]{0,1:T(8,128)(2,1)}, bf16[16384,128]{0,1:T(8,128)(2,1)}) fusion(bf16[16384,256]{0,1:T(8,128)(2,1)} %all-gather.7.cloned.1.call-done), kind=kLoop, calls=%fused_computation.83 | loop fusion | bytes 16777216 | tf_op jit(solution)/shard_map/split | solution.py:41
  362.8 58.6 %while.15 = (s32[]{:T(128)}, f32[2,256]{1,0:T(2,128)S(1)}, f32[2,256]{1,0:T(2,128)S(1)}, f32[2,256,64]{1,2,0:T(8,128)S(1)}, s32[8]{0:T(128)S(1)}, /*index=5*/s32...) while((s32[]{:T(128)}, f32[2,256]{1,0:T(2,128)S(1)}, ...), condition=%wide.region_8.9_spmd.clone, body=%wide.region_3.8_spmd.clone.sunk | while | flops 278465792 | bytes 17209772 | solution.py:244
  364.0 6.1 %conditional.3 = ((f32[2,256]{1,0:T(2,128)S(1)}, f32[2,256]{1,0:T(2,128)S(1)}, f32[2,256,64]{1,2,0:T(8,128)S(1)})) conditional(s32[]{:T(128)} %convert_element_type.113, (f32[2,256]{1,0:T(2,128)S(1)}, f32[2,256]{1,0:T(2,128)S(1)}, f32[2,256,64]{1,2,0:T(8,128)S(1)}) %tuple.39, (s32[]{:T(128)}, s32[]{:T(128)}, s32[]{:T(128)}, ...), branch_computations={%region_4.4_spmd, %region_5.7_spmd} | conditional | flops 278465792 | bytes 17208448 | solution.py:242
  367.3 1.4 fusion.47
  371.4 6.1 %conditional.3 = ((f32[2,256]{1,0:T(2,128)S(1)}, f32[2,256]{1,0:T(2,128)S(1)}, f32[2,256,64]{1,2,0:T(8,128)S(1)})) conditional(s32[]{:T(128)} %convert_element_type.113, (f32[2,256]{1,0:T(2,128)S(1)}, f32[2,256]{1,0:T(2,128)S(1)}, f32[2,256,64]{1,2,0:T(8,128)S(1)}) %tuple.39, (s32[]{:T(128)}, s32[]{:T(128)}, s32[]{:T(128)}, ...), branch_computations={%region_4.4_spmd, %region_5.7_spmd} | conditional | flops 278465792 | bytes 17208448 | solution.py:242
  374.6 1.4 fusion.47
  378.7 6.0 %conditional.3 = ((f32[2,256]{1,0:T(2,128)S(1)}, f32[2,256]{1,0:T(2,128)S(1)}, f32[2,256,64]{1,2,0:T(8,128)S(1)})) conditional(s32[]{:T(128)} %convert_element_type.113, (f32[2,256]{1,0:T(2,128)S(1)}, f32[2,256]{1,0:T(2,128)S(1)}, f32[2,256,64]{1,2,0:T(8,128)S(1)}) %tuple.39, (s32[]{:T(128)}, s32[]{:T(128)}, s32[]{:T(128)}, ...), branch_computations={%region_4.4_spmd, %region_5.7_spmd} | conditional | flops 278465792 | bytes 17208448 | solution.py:242
  386.0 6.1 %conditional.3 = ((f32[2,256]{1,0:T(2,128)S(1)}, f32[2,256]{1,0:T(2,128)S(1)}, f32[2,256,64]{1,2,0:T(8,128)S(1)})) conditional(s32[]{:T(128)} %convert_element_type.113, (f32[2,256]{1,0:T(2,128)S(1)}, f32[2,256]{1,0:T(2,128)S(1)}, f32[2,256,64]{1,2,0:T(8,128)S(1)}) %tuple.39, (s32[]{:T(128)}, s32[]{:T(128)}, s32[]{:T(128)}, ...), branch_computations={%region_4.4_spmd, %region_5.7_spmd} | conditional | flops 278465792 | bytes 17208448 | solution.py:242
  389.3 1.4 fusion.47
  393.4 6.0 %conditional.3 = ((f32[2,256]{1,0:T(2,128)S(1)}, f32[2,256]{1,0:T(2,128)S(1)}, f32[2,256,64]{1,2,0:T(8,128)S(1)})) conditional(s32[]{:T(128)} %convert_element_type.113, (f32[2,256]{1,0:T(2,128)S(1)}, f32[2,256]{1,0:T(2,128)S(1)}, f32[2,256,64]{1,2,0:T(8,128)S(1)}) %tuple.39, (s32[]{:T(128)}, s32[]{:T(128)}, s32[]{:T(128)}, ...), branch_computations={%region_4.4_spmd, %region_5.7_spmd} | conditional | flops 278465792 | bytes 17208448 | solution.py:242
  400.7 6.1 %conditional.3 = ((f32[2,256]{1,0:T(2,128)S(1)}, f32[2,256]{1,0:T(2,128)S(1)}, f32[2,256,64]{1,2,0:T(8,128)S(1)})) conditional(s32[]{:T(128)} %convert_element_type.113, (f32[2,256]{1,0:T(2,128)S(1)}, f32[2,256]{1,0:T(2,128)S(1)}, f32[2,256,64]{1,2,0:T(8,128)S(1)}) %tuple.39, (s32[]{:T(128)}, s32[]{:T(128)}, s32[]{:T(128)}, ...), branch_computations={%region_4.4_spmd, %region_5.7_spmd} | conditional | flops 278465792 | bytes 17208448 | solution.py:242
  403.9 1.4 fusion.47
  408.0 6.0 %conditional.3 = ((f32[2,256]{1,0:T(2,128)S(1)}, f32[2,256]{1,0:T(2,128)S(1)}, f32[2,256,64]{1,2,0:T(8,128)S(1)})) conditional(s32[]{:T(128)} %convert_element_type.113, (f32[2,256]{1,0:T(2,128)S(1)}, f32[2,256]{1,0:T(2,128)S(1)}, f32[2,256,64]{1,2,0:T(8,128)S(1)}) %tuple.39, (s32[]{:T(128)}, s32[]{:T(128)}, s32[]{:T(128)}, ...), branch_computations={%region_4.4_spmd, %region_5.7_spmd} | conditional | flops 278465792 | bytes 17208448 | solution.py:242
  415.3 6.0 %conditional.3 = ((f32[2,256]{1,0:T(2,128)S(1)}, f32[2,256]{1,0:T(2,128)S(1)}, f32[2,256,64]{1,2,0:T(8,128)S(1)})) conditional(s32[]{:T(128)} %convert_element_type.113, (f32[2,256]{1,0:T(2,128)S(1)}, f32[2,256]{1,0:T(2,128)S(1)}, f32[2,256,64]{1,2,0:T(8,128)S(1)}) %tuple.39, (s32[]{:T(128)}, s32[]{:T(128)}, s32[]{:T(128)}, ...), branch_computations={%region_4.4_spmd, %region_5.7_spmd} | conditional | flops 278465792 | bytes 17208448 | solution.py:242
  421.9 22.0 %all_to_all.16 = bf16[4,64,2048]{2,1,0:T(8,128)(2,1)S(1)} all-to-all(bf16[4,64,2048]{2,1,0:T(8,128)(2,1)S(1)} %bitcast.69), channel_id=1, replica_groups=mesh['grp'=2,'sp_0'=32,'sp_1'=2,'tp'=4] {'tp'}, dimensions={0} | all-to-all | bytes 2097152 | tf_op jit(solution)/shard_map/all_to_all | solution.py:76
  (157 shorter events, 55.8 us)
Async XLA Ops:
  6.5 22.7 %copy-start.1 = (f32[2048]{0:T(1024)S(1)}, f32[2048]{0:T(1024)}, u32[]{:S(2)}) copy-start(f32[2048]{0:T(1024)} %param.19) | copy-start | bytes 24580
  6.5 122.5 %all-gather.5.cloned.1.call-start = ((), (), s32[]{:S(2)}) async-start(), calls=%async_computation.3 | async-start | bytes 2662400 | tf_op jit(solution)/shard_map/all_gather | solution.py:40
  8.1 348.8 %all-gather.7.cloned.1.call-start = ((), (), s32[]{:S(2)}) async-start(), calls=%async_computation.4 | async-start | bytes 8519680 | tf_op jit(solution)/shard_map/all_gather | solution.py:40
  29.2 103.4 %copy-start.2 = (bf16[128,32]{0,1:T(8,128)(2,1)S(1)}, bf16[128,32]{0,1:T(8,128)(2,1)}, u32[]{:S(2)}) copy-start(bf16[128,32]{0,1:T(8,128)(2,1)} %param.31) | copy-start | bytes 24580
  29.2 103.4 %copy-start.3 = (bf16[128,32]{0,1:T(8,128)(2,1)S(1)}, bf16[128,32]{0,1:T(8,128)(2,1)}, u32[]{:S(2)}) copy-start(bf16[128,32]{0,1:T(8,128)(2,1)} %param.30) | copy-start | bytes 24580
  130.5 20.7 %copy-start.5 = (f32[128]{0:T(128)S(1)}, f32[128]{0:T(128)}, u32[]{:S(2)}) copy-start(f32[128]{0:T(128)} %param.28) | copy-start | bytes 1540
  130.5 20.8 %copy-start.4 = (f32[2]{0:T(128)S(1)}, f32[2]{0:T(128)}, u32[]{:S(2)}) copy-start(f32[2]{0:T(128)} %param.26) | copy-start | bytes 28
  133.8 176.3 %all-to-all-start.1 = ((bf16[64,32,256]{2,1,0:T(8,128)(2,1)}), bf16[64,32,256]{2,1,0:T(8,128)(2,1)S(1)}, u32[]{:S(2)}, u32[]{:S(2)}) async-start(bf16[64,32,256]{2,1,0:T(8,128)(2,1)} %stack.2), calls=%async_computation.1 | async-start | bytes 2097152 | tf_op jit(solution)/shard_map/all_to_all | solution.py:16
  305.7 2.1 copy-start
Sparse Core Ops, SparseCore 0:
  9.5 119.5 all-gather.4
  132.7 224.1 all-gather.6
